TPU v7x, 32 devices: a whole 2x2x4 slice. The times are simulated.
32 devices in a mesh: ep: 4 (over y, x), tp: 8 (over z, core).
Axes of the slice: x: 2, y: 2, z: 4, core: 2. Of those that a mesh axis runs over, the one named last changes fastest.
Arguments:
- pool_input: bfloat16 [4096, 1024], P('ep', 'tp'), may hold values from -6 to 6
- pool_gain: float32 [1024], P('tp'), may hold values from 0.1 to 1.9
- mix_weight: bfloat16 [1024, 2048], P('tp'), may hold values from -0.1875 to 0.1875
- moe_input: bfloat16 [8192, 2048], P(('ep', 'tp')), may hold values from -6 to 6
- moe_gain: float32 [2048], replicated, may hold values from 0.1 to 1.9
- expert_ids: int32 [8192, 2], P(('ep', 'tp')), may hold values from 0 to 15, as said below
- route_weight: float32 [8192, 2], P(('ep', 'tp')), may hold values from 0.2 to 1
- gate_weight: bfloat16 [16, 2048, 1024], P('ep', None, 'tp'), may hold values from -0.125 to 0.125
- up_weight: bfloat16 [16, 2048, 1024], P('ep', None, 'tp'), may hold values from -0.125 to 0.125
- down_weight: bfloat16 [16, 2048, 1024], P('ep', None, 'tp'), may hold values from -0.1875 to 0.1875
Outputs:
- mixed_out: bfloat16 [4096, 2048], P(('ep', 'tp'))
- moe_out: bfloat16 [8192, 2048], P(('ep', 'tp'))
Inputs may be any that keep to these rules, and one draw needn't show every extreme that they name: `expert_ids`: each row names 2 different experts of one group of 4 consecutive experts. In each aligned block of 256 rows (the rows of one device) no expert is named by more than 48 rows, and some expert is named by exactly 48 rows.
All inputs are finite; a program needn't handle non-finite values.
Results may differ from a plain program's by a relative error of at most 0.012.
Values may be sent and summed in bfloat16 or wider, within the bound.
A program may use at most 128 MiB of HBM per device.

v0:
```python
import jax
import jax.numpy as jnp
from jax import lax
from jax.sharding import PartitionSpec as P

GROUP_CH = 256
EXPERTS = 16
TOP = 2
CAP = 48
eps_norm = 1e-06


def from_behind(shard, axis, by):
    peers = lax.axis_size(axis)
    pairs = [(i, i + by) for i in range(peers) if 0 <= i + by < peers]
    return lax.ppermute(shard, axis, pairs)


def window_sums(extended, row_count):
    level_sum = extended
    stride = 1
    outputs = []
    for doubling in range(4):
        level_sum = level_sum[stride:] + level_sum[:-stride]
        stride = stride * 2
        outputs.append(level_sum[level_sum.shape[0] - row_count :])
    return outputs


def pool_mixer(pool_input, pool_gain):
    row_count, channels = pool_input.shape
    carried = from_behind(pool_input[row_count - 15 :], "ep", 1)
    extended = jnp.concatenate([carried, pool_input], axis=0).astype(jnp.float32)
    window_list = window_sums(extended, row_count)
    channel_ids = lax.axis_index("tp") * channels + lax.iota(jnp.int32, channels)
    group_ids = channel_ids // GROUP_CH
    position = lax.axis_index("ep") * row_count + lax.iota(jnp.int32, row_count)
    summed = jnp.zeros((row_count, channels), jnp.float32)
    widths = jnp.zeros((channels,), jnp.int32)
    for index_group in range(4):
        inside = group_ids == index_group
        summed = jnp.where(inside[None, :], window_list[index_group], summed)
        widths = jnp.where(inside, 2 ** (index_group + 1), widths)
    counted = jnp.minimum(position[:, None] + 1, widths[None, :]).astype(jnp.float32)
    values = extended[15:]
    return ((summed / counted - values) * pool_gain).astype(jnp.bfloat16)


def route_slots(expert_ids):
    flat_ids = expert_ids.reshape(-1)
    marked = (flat_ids[:, None] == lax.iota(jnp.int32, EXPERTS)[None, :]).astype(jnp.int32)
    before_count = jnp.cumsum(marked, axis=0) - marked
    ranked = jnp.sum(before_count * marked, axis=1)
    return (flat_ids * CAP + ranked).reshape(expert_ids.shape)


def body(
    pool_input,
    pool_gain,
    mix_weight,
    moe_input,
    moe_gain,
    expert_ids,
    route_weight,
    gate_weight,
    up_weight,
    down_weight,
):
    pooled = pool_mixer(pool_input, pool_gain)
    regrouped = lax.all_to_all(pooled, "tp", split_axis=0, concat_axis=1, tiled=True)
    mixed_sum = jnp.dot(
        regrouped,
        lax.all_gather(mix_weight, "tp", axis=0, tiled=True),
        preferred_element_type=jnp.float32,
    )
    mixed_out = mixed_sum.astype(jnp.bfloat16)
    inputs = moe_input.astype(jnp.float32)
    scale_rows = lax.rsqrt(jnp.mean(inputs * inputs, axis=-1, keepdims=True) + eps_norm)
    normed = (inputs * scale_rows * moe_gain).astype(jnp.bfloat16)
    slots = route_slots(expert_ids)
    slot_index = lax.iota(jnp.int32, EXPERTS * CAP)
    placing = (
        (slot_index[:, None] == slots[None, :, 0]) | (slot_index[:, None] == slots[None, :, 1])
    ).astype(jnp.bfloat16)
    outgoing = jnp.dot(placing, normed, preferred_element_type=jnp.float32).astype(jnp.bfloat16)
    outgoing = outgoing.reshape(EXPERTS, CAP, normed.shape[1])
    arrived = lax.all_to_all(outgoing, "ep", split_axis=0, concat_axis=1, tiled=True)
    gate_piece = lax.all_gather(gate_weight, "tp", axis=2, tiled=True)
    up_piece = lax.all_gather(up_weight, "tp", axis=2, tiled=True)
    down_piece = lax.all_gather(down_weight, "tp", axis=2, tiled=True)
    gate_part = jnp.einsum("erd,edf->erf", arrived, gate_piece, preferred_element_type=jnp.float32)
    upward = jnp.einsum("erd,edf->erf", arrived, up_piece, preferred_element_type=jnp.float32)
    hidden = (jax.nn.silu(gate_part) * upward).astype(jnp.bfloat16)
    expert_sum = jnp.einsum("erf,edf->erd", hidden, down_piece, preferred_element_type=jnp.float32)
    expert_rows = expert_sum.astype(jnp.bfloat16)
    returned = lax.all_to_all(expert_rows, "ep", split_axis=1, concat_axis=0, tiled=True)
    returned_rows = returned.reshape(EXPERTS * CAP, returned.shape[2])
    combined = jnp.zeros((normed.shape[0], normed.shape[1]), jnp.float32)
    for route_index in range(TOP):
        picking = (slots[:, route_index][:, None] == slot_index[None, :]).astype(jnp.bfloat16)
        chosen_rows = jnp.dot(picking, returned_rows, preferred_element_type=jnp.float32)
        combined = combined + route_weight[:, route_index : route_index + 1] * chosen_rows
    moe_out = combined.astype(jnp.bfloat16)
    return (mixed_out, moe_out)


def solution(mesh):
    return jax.shard_map(
        body,
        mesh=mesh,
        in_specs=(
            P("ep", "tp"),
            P("tp"),
            P("tp", None),
            P(("ep", "tp"), None),
            P(),
            P(("ep", "tp"), None),
            P(("ep", "tp"), None),
            P("ep", None, "tp"),
            P("ep", None, "tp"),
            P("ep", None, "tp"),
        ),
        out_specs=(P(("ep", "tp"), None), P(("ep", "tp"), None)),
        check_vma=False,
    )
```

profile of v0, /device:TPU:0, one launch (start us, length us, event | category | flops | bytes accessed | tf_op | source)
XLA Modules:
  0.0 554.3 jit_solution(15557223583954882724)
XLA Ops:
  7.2 0.7 all-gather.7.cloned.1.call-update
  8.0 0.7 all-gather.11.cloned.1.call-update
  8.7 0.7 all-gather.9.cloned.1.call-update
  9.6 0.1 eq.138
  9.9 1.2 reduce-window.6
  11.0 0.2 slice_reduce_fusion
  11.4 0.1 reduce_sum.21
  11.6 0.3 fusion.2
  12.0 2.8 convolution_convert_fusion
  14.7 5.3 all-to-all-start.1
  20.1 3.9 collective-permute-start
  24.1 30.0 %collective-permute-done = bf16[15,128]{1,0:T(8,128)(2,1)S(1)} collective-permute-done((bf16[15,128]{1,0:T(8,128)(2,1)S(1)}, bf16[15,128]{1,0:T(8,128)(2,1)S(1)}, u32[]{:S(2)}, u32[]{:S(2)}) %collective-permute-start) | collective-permute-done | bytes 3872 | tf_op jit(solution)/shard_map/ppermute | solution.py:16
  54.4 1.1 fusion.12
  55.4 0.8 all-to-all-done.1
  56.2 5.2 all-to-all-start
  61.4 1.9 copy.51
  63.3 107.9 %all-gather.7.cloned.1.call-done = bf16[4,2048,1024]{2,1,0:T(8,128)(2,1)} async-done(((bf16[4,2048,128]{2,1,0:T(8,128)(2,1)}), bf16[4,2048,1024]{2,1,0:T(8,128)(2,1)}) %all-gather.7.cloned.1.call-update) | async-done | bytes 16777232 | tf_op jit(solution)/shard_map/all_gather | solution.py:88
  171.2 11.9 %fusion.28 = f32[4,192,1024]{2,1,0:T(8,128)} fusion(bf16[4,192,2048]{2,1,0:T(8,128)(2,1)} %bitcast.48, bf16[4,2048,1024]{2,1,0:T(8,128)(2,1)} %all-gather.7.cloned.1.call-done), kind=kOutput, calls=%fused_computation.62 | convolution fusion | flops 3221225472 | bytes 23068672 | tf_op jit(solution)/shard_map/erd,edf->erf/dot_general | solution.py:91
  183.2 142.6 %all-gather.11.cloned.1.call-done = bf16[4,2048,1024]{2,1,0:T(8,128)(2,1)} async-done(((bf16[4,2048,128]{2,1,0:T(8,128)(2,1)}), bf16[4,2048,1024]{2,1,0:T(8,128)(2,1)}) %all-gather.11.cloned.1.call-update) | async-done | bytes 16777232 | tf_op jit(solution)/shard_map/all_gather | solution.py:90
  325.8 151.6 %all-gather.9.cloned.1.call-done = bf16[4,2048,1024]{2,1,0:T(8,128)(2,1)} async-done(((bf16[4,2048,128]{2,1,0:T(8,128)(2,1)}), bf16[4,2048,1024]{2,1,0:T(8,128)(2,1)}) %all-gather.9.cloned.1.call-update) | async-done | bytes 16777232 | tf_op jit(solution)/shard_map/all_gather | solution.py:89
  477.4 17.7 %convolution_convert_fusion.1 = bf16[4,192,2048]{2,1,0:T(8,128)(2,1)} fusion(bf16[4,2048,1024]{2,1,0:T(8,128)(2,1)} %all-gather.11.cloned.1.call-done, f32[4,192,1024]{2,1,0:T(8,128)} %fusion.28, bf16[4,192,2048]{2,1,0:T(8,128)(2,1)S(1)} %bitcast.49, bf16[4,2048,1024]{2,1,0:T(8,128)(2,1)} %all-gather.9.cloned.1.call-done), kind=kOutput, calls=%fused_computation.1 | convolution fusion | flops 6448742400 | bytes 42991616 | tf_op jit(solution)/shard_map/erf,edf->erd/dot_general | solution.py:94
  495.1 6.0 %copy.52 = bf16[4,192,2048]{2,0,1:T(4,128)(2,1)} copy(bf16[4,192,2048]{2,1,0:T(8,128)(2,1)} %convolution_convert_fusion.1) | data formatting | bytes 6291456 | tf_op jit(solution)/shard_map/convert_element_type | solution.py:95
  501.1 0.7 copy-done.2
  501.8 3.9 all-to-all-start.2
  505.7 1.1 copy.46
  506.9 17.0 %all-gather.5.cloned.1.call-done = bf16[1024,2048]{1,0:T(8,128)(2,1)} async-done(((bf16[128,2048]{1,0:T(8,128)(2,1)}), bf16[1024,2048]{1,0:T(8,128)(2,1)}) %all-gather.5.cloned.1.call-update) | async-done | bytes 4194320 | tf_op jit(solution)/shard_map/all_gather | solution.py:73
  523.9 3.7 convolution_convert_fusion.2
  527.6 14.8 %all-to-all-done.2 = bf16[4,192,2048]{2,0,1:T(4,128)(2,1)S(1)} async-done(((bf16[4,192,2048]{2,0,1:T(4,128)(2,1)}), bf16[4,192,2048]{2,0,1:T(4,128)(2,1)S(1)}, u32[]{:S(2)}, u32[]{:S(2)}) %all-to-all-start.2) | async-done | bytes 3145760 | tf_op jit(solution)/shard_map/all_to_all | solution.py:96
  542.5 1.7 copy.53
  544.2 0.4 copy.54
  544.6 1.0 convolution_multiply_fusion.1
  545.7 2.1 fusion.1
  (41 shorter events, 1.0 us)
Async XLA Ops:
  7.2 2.3 copy-start.5
  7.2 4.4 copy-start.1
  7.2 164.1 %all-gather.7.cloned.1.call-start = ((), (), s32[]{:S(2)}) async-start(), calls=%async_computation.4 | async-start | bytes 18874368 | tf_op jit(solution)/shard_map/all_gather | solution.py:88
  7.9 4.0 copy-start.4
  7.9 317.8 %all-gather.11.cloned.1.call-start = ((), (), s32[]{:S(2)}) async-start(), calls=%async_computation.6 | async-start | bytes 18874368 | tf_op jit(solution)/shard_map/all_gather | solution.py:90
  8.7 468.7 %all-gather.9.cloned.1.call-start = ((), (), s32[]{:S(2)}) async-start(), calls=%async_computation.5 | async-start | bytes 18874368 | tf_op jit(solution)/shard_map/all_gather | solution.py:89
  14.7 5.3 copy-start.3
  14.7 41.5 %all-to-all-start.1 = ((bf16[16,48,2048]{2,1,0:T(8,128)(2,1)}), bf16[16,48,2048]{2,1,0:T(8,128)(2,1)S(1)}, u32[]{:S(2)}, u32[]{:S(2)}) async-start(bf16[16,48,2048]{2,1,0:T(8,128)(2,1)} %bitcast.7), calls=%async_computation.1 | async-start | bytes 6291456 | tf_op jit(solution)/shard_map/all_to_all | solution.py:87
  20.0 34.3 %copy-start.7 = (f32[128]{0:T(128)S(1)}, f32[128]{0:T(128)}, u32[]{:S(2)}) copy-start(f32[128]{0:T(128)} %param.11) | copy-start | bytes 1540
  20.0 503.9 %all-gather.5.cloned.1.call-start = ((), (), s32[]{:S(2)}) async-start(), calls=%async_computation.3 | async-start | bytes 4718592 | tf_op jit(solution)/shard_map/all_gather | solution.py:73
  20.1 34.0 %collective-permute-start = (bf16[15,128]{1,0:T(8,128)(2,1)S(1)}, bf16[15,128]{1,0:T(8,128)(2,1)S(1)}, u32[]{:S(2)}, u32[]{:S(2)}) collective-permute-start(bf16[15,128]{1,0:T(8,128)(2,1)S(1)} %slice.57), channel_id=1, source_target_pairs={{0,8},{8,16},{16,24},{1,9},{9,17},{17,25},{2,10},{10,18},{18,26},{... | collective-permute-start | bytes 11528 | tf_op jit(solution)/shard_map/ppermute | solution.py:16
  56.2 444.9 %all-to-all-start = ((bf16[8,128,128]{2,1,0:T(8,128)(2,1)}), bf16[8,128,128]{2,1,0:T(8,128)(2,1)S(1)}, u32[]{:S(2)}, u32[]{:S(2)}) async-start(bf16[8,128,128]{2,1,0:T(8,128)(2,1)} %bitcast), calls=%async_computation | async-start | bytes 524288 | tf_op jit(solution)/shard_map/all_to_all | solution.py:70
  171.2 306.1 %copy-start = (bf16[4,4,48,2048]{3,2,0,1:T(8,128)(2,1)S(1)}, bf16[4,4,48,2048]{3,2,0,1:T(8,128)(2,1)}, u32[]{:S(2)}) copy-start(bf16[4,4,48,2048]{3,2,0,1:T(8,128)(2,1)} %copy.51) | copy-start | bytes 9437188
  501.1 4.6 copy-start.6
  501.1 0.7 copy-start.2
  501.8 40.6 %all-to-all-start.2 = ((bf16[4,192,2048]{2,0,1:T(4,128)(2,1)}), bf16[4,192,2048]{2,0,1:T(4,128)(2,1)S(1)}, u32[]{:S(2)}, u32[]{:S(2)}) async-start(bf16[4,192,2048]{2,0,1:T(4,128)(2,1)} %copy.52), calls=%async_computation.2 | async-start | bytes 6291456 | tf_op jit(solution)/shard_map/all_to_all | solution.py:96
Sparse Core Ops, SparseCore 0:
  9.6 161.6 all-gather.6
  172.8 152.8 all-gather.10
  327.4 149.9 all-gather.8
  478.8 45.0 all-gather.4
where the time goes:
time: 555 us; the launch traced here: 554 us
  waiting for transfers between devices  467 us (84%)
  matrix products  39.2 us (7%)
  starting transfers between devices  18.4 us (3%)
  between operations  14 us (3%)
  local copies, waits for them, and re-layouts  12.8 us (2%)
    all_gather x1, waiting for transfers between devices, body(): up_piece = lax.all_gather(up_weight, 'tp', axis=2, tiled=True)  152 us
    all_gather x1, waiting for transfers between devices, body(): down_piece = lax.all_gather(down_weight, 'tp', axis=2, tiled=True)  143 us
    all_gather x1, waiting for transfers between devices, body(): gate_piece = lax.all_gather(gate_weight, 'tp', axis=2, tiled=True)  108 us
    ppermute x1, waiting for transfers between devices, from_behind(): return lax.ppermute(shard, axis, pairs)  30 us
    dot_general x1, matrix products, body(): jnp.einsum('erf,edf->erd', hidden, down_piece, preferred_element_type=jnp...  17.7 us
    all_gather x1, waiting for transfers between devices, body(): lax.all_gather(mix_weight, 'tp', axis=0, tiled=True)  17 us
    all_to_all x1, waiting for transfers between devices, body(): lax.all_to_all(expert_rows, 'ep', split_axis=1, concat_axis=0, tiled=True)  14.8 us
    dot_general x1, matrix products, body(): jnp.einsum('erd,edf->erf', arrived, gate_piece, preferred_element_type=jn...  11.9 us
  transfers between devices with their start and end apart: 8, of which 7 were waited for; matrix products, arithmetic and copies ran while one was open for 9% of the time, Pallas kernels for 0%

commit v1 on v0

--- a/solution.py
+++ b/solution.py
@@ -8,6 +8,31 @@
 TOP = 2
 CAP = 48
 eps_norm = 1e-06
+
+
+def joined_along(blocks, dim):
+    dims = list(blocks.shape[1:])
+    dims[dim] *= blocks.shape[0]
+    return jnp.moveaxis(blocks, 0, dim).reshape(dims)
+
+
+def ring_apply(value, axis, dim, apply, out_dim):
+    peers, index, span = (lax.axis_size(axis), lax.axis_index(axis), value.shape[dim])
+    right = [(i, (i + 1) % peers) for i in range(peers)]
+    left = [(i, (i - 1) % peers) for i in range(peers)]
+    half = peers // 2
+    tiles = {}
+    from_left = from_right = value
+    for turn in range(half + 1):
+        next_left = lax.ppermute(from_left, axis, right) if turn < half else None
+        next_right = lax.ppermute(from_right, axis, left) if turn < peers - half - 1 else None
+        tiles[-turn] = apply(from_left, (index - turn) % peers * span)
+        if 0 < turn < peers - half:
+            tiles[turn] = apply(from_right, (index + turn) % peers * span)
+        from_left, from_right = (next_left, next_right)
+    tiles = jnp.stack([tiles[k] for k in sorted(tiles)])
+    tiles = tiles[(jnp.arange(peers) - index + half) % peers]
+    return joined_along(tiles, out_dim)
 
 
 def from_behind(shard, axis, by):
@@ -86,10 +111,17 @@
     outgoing = outgoing.reshape(EXPERTS, CAP, normed.shape[1])
     arrived = lax.all_to_all(outgoing, "ep", split_axis=0, concat_axis=1, tiled=True)
     gate_piece = lax.all_gather(gate_weight, "tp", axis=2, tiled=True)
-    up_piece = lax.all_gather(up_weight, "tp", axis=2, tiled=True)
     down_piece = lax.all_gather(down_weight, "tp", axis=2, tiled=True)
     gate_part = jnp.einsum("erd,edf->erf", arrived, gate_piece, preferred_element_type=jnp.float32)
-    upward = jnp.einsum("erd,edf->erf", arrived, up_piece, preferred_element_type=jnp.float32)
+    upward = ring_apply(
+        up_weight,
+        "tp",
+        2,
+        lambda shard_2, at: jnp.einsum(
+            "erd,edf->erf", arrived, shard_2, preferred_element_type=jnp.float32
+        ),
+        2,
+    )
     hidden = (jax.nn.silu(gate_part) * upward).astype(jnp.bfloat16)
     expert_sum = jnp.einsum("erf,edf->erd", hidden, down_piece, preferred_element_type=jnp.float32)
     expert_rows = expert_sum.astype(jnp.bfloat16)

time: 555 us -> 536 us (0.966)
  waiting for transfers between devices: 467 us -> 377 us
  starting transfers between devices: 18.4 us -> 73.9 us
  matrix products: 39.2 us -> 51.1 us
    ppermute x0 -> x7, waiting for transfers between devices: none -> 241 us  [the longest x4 203 us: ring_apply(): next_left = lax.ppermute(from_left, axis, right) if turn < half else None]
    all_gather x1 -> x0, waiting for transfers between devices: 152 us -> none  [body(): up_piece = lax.all_gather(up_weight, 'tp', axis=2, tiled=True)]
    all_gather x1, waiting for transfers between devices: 108 us -> 0.01 us  [body(): gate_piece = lax.all_gather(gate_weight, 'tp', axis=2, tiled=True)]
    all_gather x1, waiting for transfers between devices: 143 us -> 102 us  [body(): down_piece = lax.all_gather(down_weight, 'tp', axis=2, tiled=True)]
    ppermute x0 -> x7, starting transfers between devices: none -> 36 us  [the longest x4 30.2 us: ring_apply(): next_left = lax.ppermute(from_left, axis, right) if turn < half else None]
    ppermute x1, waiting for transfers between devices: 30 us -> 0.01 us  [from_behind(): return lax.ppermute(shard, axis, pairs)]
    all_to_all x1, starting transfers between devices: 5.19 us -> 26.5 us  [body(): lax.all_to_all(pooled, 'tp', split_axis=0, concat_axis=1, tiled=True)]
    dot_general x1 -> x8, matrix products: 11.9 us -> 23.7 us  [body(): jnp.einsum('erd,edf->erf', arrived, shard_2, preferred_element_type=jnp.f...]
  transfers between devices with their start and end apart: 8 -> 14, of which waited for: 7 -> 8; matrix products, arithmetic and copies ran while one was open for 9% -> 12% of each run, Pallas kernels for 0% -> 0%
where the time goes in v1:
time: 536 us; the launch traced here: 534 us
  waiting for transfers between devices  377 us (70%)
  starting transfers between devices  73.9 us (14%)
  matrix products  51.1 us (10%)
  local copies, waits for them, and re-layouts  15.7 us (3%)
  between operations  14 us (3%)
    ppermute x4, waiting for transfers between devices, ring_apply(): next_left = lax.ppermute(from_left, axis, right) if turn < half else None  203 us
    all_gather x1, waiting for transfers between devices, body(): down_piece = lax.all_gather(down_weight, 'tp', axis=2, tiled=True)  102 us
    ppermute x3, waiting for transfers between devices, ring_apply(): lax.ppermute(from_right, axis, left)  38.4 us
    ppermute x4, starting transfers between devices, ring_apply(): next_left = lax.ppermute(from_left, axis, right) if turn < half else None  30.2 us
    all_to_all x1, starting transfers between devices, body(): lax.all_to_all(pooled, 'tp', split_axis=0, concat_axis=1, tiled=True)  26.5 us
    dot_general x8, matrix products, body(): jnp.einsum('erd,edf->erf', arrived, shard_2, preferred_element_type=jnp.f...  23.7 us
    all_gather x1, waiting for transfers between devices, body(): lax.all_gather(mix_weight, 'tp', axis=0, tiled=True)  21.5 us
    dot_general x1, matrix products, body(): jnp.einsum('erf,edf->erd', hidden, down_piece, preferred_element_type=jnp...  17.8 us
  transfers between devices with their start and end apart: 14, of which 8 were waited for; matrix products, arithmetic and copies ran while one was open for 12% of the time, Pallas kernels for 0%

profile of v1, /device:TPU:0, one launch (start us, length us, event | category | flops | bytes accessed | tf_op | source)
XLA Modules:
  0.0 534.3 jit_solution(13503935739335874954)
XLA Ops:
  9.2 49.7 %collective-permute-done.1 = bf16[4,2048,128]{2,1,0:T(8,128)(2,1)S(1)} collective-permute-done((bf16[4,2048,128]{2,1,0:T(8,128)(2,1)}, bf16[4,2048,128]{2,1,0:T(8,128)(2,1)S(1)}, u32[]{:S(2)}, u32[]{:S(2)}) %collective-permute-start.1) | collective-permute-done | bytes 2097184 | tf_op jit(solution)/shard_map/ppermute | solution.py:27
  58.9 1.6 collective-permute-start.2
  60.5 2.0 collective-permute-start.5
  62.9 79.9 %collective-permute-done.2 = bf16[4,2048,128]{2,1,0:T(8,128)(2,1)} collective-permute-done((bf16[4,2048,128]{2,1,0:T(8,128)(2,1)S(1)}, bf16[4,2048,128]{2,1,0:T(8,128)(2,1)}, u32[]{:S(2)}, u32[]{:S(2)}) %collective-permute-start.2) | collective-permute-done | bytes 2097184 | tf_op jit(solution)/shard_map/ppermute | solution.py:27
  142.8 10.4 %collective-permute-start.3 = (bf16[4,2048,128]{2,1,0:T(8,128)(2,1)}, bf16[4,2048,128]{2,1,0:T(8,128)(2,1)}, u32[]{:S(2)}, u32[]{:S(2)}) collective-permute-start(bf16[4,2048,128]{2,1,0:T(8,128)(2,1)} %collective-permute-done.2), channel_id=1, source_target_pairs={{0,1},{1,2},{2,3},{3,4},{4,5},{5,6},{6,7},{7,0},{8,9},{9,10},{10,1... | collective-permute-start | bytes 6291464 | tf_op jit(solution)/shard_map/ppermute | solution.py:27
  155.3 2.7 convolution_convert_fusion
  158.1 3.8 all-to-all-start.1
  162.0 3.8 collective-permute-start
  166.0 59.4 %collective-permute-done.3 = bf16[4,2048,128]{2,1,0:T(8,128)(2,1)} collective-permute-done((bf16[4,2048,128]{2,1,0:T(8,128)(2,1)}, bf16[4,2048,128]{2,1,0:T(8,128)(2,1)}, u32[]{:S(2)}, u32[]{:S(2)}) %collective-permute-start.3) | collective-permute-done | bytes 2097184 | tf_op jit(solution)/shard_map/ppermute | solution.py:27
  225.5 17.6 %collective-permute-start.4 = (bf16[4,2048,128]{2,1,0:T(8,128)(2,1)}, bf16[4,2048,128]{2,1,0:T(8,128)(2,1)}, u32[]{:S(2)}, u32[]{:S(2)}) collective-permute-start(bf16[4,2048,128]{2,1,0:T(8,128)(2,1)} %collective-permute-done.3), channel_id=1, source_target_pairs={{0,1},{1,2},{2,3},{3,4},{4,5},{5,6},{6,7},{7,0},{8,9},{9,10},{10,1... | collective-permute-start | bytes 6291464 | tf_op jit(solution)/shard_map/ppermute | solution.py:27
  244.5 26.5 %all-to-all-start = ((bf16[8,128,128]{2,1,0:T(8,128)(2,1)}), bf16[8,128,128]{2,1,0:T(8,128)(2,1)S(1)}, u32[]{:S(2)}, u32[]{:S(2)}) async-start(bf16[8,128,128]{2,1,0:T(8,128)(2,1)} %bitcast), calls=%async_computation | async-start | bytes 524288 | tf_op jit(solution)/shard_map/all_to_all | solution.py:95
  271.2 3.8 collective-permute-start.7
  274.9 13.8 %collective-permute-done.4 = bf16[4,2048,128]{2,1,0:T(8,128)(2,1)} collective-permute-done((bf16[4,2048,128]{2,1,0:T(8,128)(2,1)}, bf16[4,2048,128]{2,1,0:T(8,128)(2,1)}, u32[]{:S(2)}, u32[]{:S(2)}) %collective-permute-start.4) | collective-permute-done | bytes 2097184 | tf_op jit(solution)/shard_map/ppermute | solution.py:27
  288.8 3.3 fusion.15
  292.1 3.3 fusion.14
  295.5 3.5 fusion.13
  298.9 1.8 fusion.12
  300.7 3.3 fusion.11
  304.0 3.3 fusion.10
  307.3 3.3 fusion.9
  310.7 38.4 %collective-permute-done.7 = bf16[4,2048,128]{2,1,0:T(8,128)(2,1)S(1)} collective-permute-done((bf16[4,2048,128]{2,1,0:T(8,128)(2,1)}, bf16[4,2048,128]{2,1,0:T(8,128)(2,1)S(1)}, u32[]{:S(2)}, u32[]{:S(2)}) %collective-permute-start.7) | collective-permute-done | bytes 2097184 | tf_op jit(solution)/shard_map/ppermute | solution.py:28
  349.1 1.8 fusion.8
  350.9 4.6 gather_fusion
  355.5 102.1 %all-gather.8.cloned.1.call-done = bf16[4,2048,1024]{2,1,0:T(8,128)(2,1)} async-done(((bf16[4,2048,128]{2,1,0:T(8,128)(2,1)}), bf16[4,2048,1024]{2,1,0:T(8,128)(2,1)}) %all-gather.8.cloned.1.call-update) | async-done | bytes 16777232 | tf_op jit(solution)/shard_map/all_gather | solution.py:114
  457.6 17.8 %convolution_convert_fusion.1 = bf16[4,192,2048]{2,1,0:T(8,128)(2,1)} fusion(bf16[4,2048,1024]{2,1,0:T(8,128)(2,1)} %all-gather.8.cloned.1.call-done, bf16[4,192,2048]{2,1,0:T(8,128)(2,1)S(1)} %bitcast.114, bf16[4,2048,1024]{2,1,0:T(8,128)(2,1)} %all-gather.6.cloned.1.call-done, f32[8,4,192,128]{3,2,1,0:T(8,128)} %gather_fusion), kind=kOutput, calls=%fused_computation.2 | convolution fusion | flops 6448742400 | bytes 42991616 | tf_op jit(solution)/shard_map/erf,edf->erd/dot_general | solution.py:126
  475.4 6.0 %copy.58 = bf16[4,192,2048]{2,0,1:T(4,128)(2,1)} copy(bf16[4,192,2048]{2,1,0:T(8,128)(2,1)} %convolution_convert_fusion.1) | data formatting | bytes 6291456 | tf_op jit(solution)/shard_map/convert_element_type | solution.py:127
  482.0 3.7 all-to-all-start.2
  486.9 21.5 %all-gather.4.cloned.1.call-done = bf16[1024,2048]{1,0:T(8,128)(2,1)} async-done(((bf16[128,2048]{1,0:T(8,128)(2,1)}), bf16[1024,2048]{1,0:T(8,128)(2,1)}) %all-gather.4.cloned.1.call-update) | async-done | bytes 4194320 | tf_op jit(solution)/shard_map/all_gather | solution.py:98
  508.4 3.7 convolution_convert_fusion.2
  512.1 10.4 %all-to-all-done.2 = bf16[4,192,2048]{2,0,1:T(4,128)(2,1)S(1)} async-done(((bf16[4,192,2048]{2,0,1:T(4,128)(2,1)}), bf16[4,192,2048]{2,0,1:T(4,128)(2,1)S(1)}, u32[]{:S(2)}, u32[]{:S(2)}) %all-to-all-start.2) | async-done | bytes 3145760 | tf_op jit(solution)/shard_map/all_to_all | solution.py:128
  522.5 1.7 copy.59
  525.7 2.1 fusion.2
  (68 shorter events, 9.5 us)
Async XLA Ops:
  7.2 55.3 %copy-start.6 = (s32[256,2]{0,1:T(2,128)S(1)}, s32[256,2]{0,1:T(2,128)}, u32[]{:S(2)}) copy-start(s32[256,2]{0,1:T(2,128)} %param.15) | copy-start | bytes 6148
  7.2 147.8 %copy-start = (bf16[256,2048]{1,0:T(8,128)(2,1)S(1)}, bf16[256,2048]{1,0:T(8,128)(2,1)}, u32[]{:S(2)}) copy-start(bf16[256,2048]{1,0:T(8,128)(2,1)} %param.13) | copy-start | bytes 3145732
  7.2 148.2 %copy-start.5 = (f32[2048]{0:T(1024)S(1)}, f32[2048]{0:T(1024)}, u32[]{:S(2)}) copy-start(f32[2048]{0:T(1024)} %param.14) | copy-start | bytes 24580
  7.2 348.3 %all-gather.6.cloned.1.call-start = ((), (), s32[]{:S(2)}) async-start(), calls=%async_computation.4 | async-start | bytes 18874368 | tf_op jit(solution)/shard_map/all_gather | solution.py:113
  7.9 449.6 %all-gather.8.cloned.1.call-start = ((), (), s32[]{:S(2)}) async-start(), calls=%async_computation.5 | async-start | bytes 18874368 | tf_op jit(solution)/shard_map/all_gather | solution.py:114
  8.7 50.3 %collective-permute-start.1 = (bf16[4,2048,128]{2,1,0:T(8,128)(2,1)}, bf16[4,2048,128]{2,1,0:T(8,128)(2,1)S(1)}, u32[]{:S(2)}, u32[]{:S(2)}) collective-permute-start(bf16[4,2048,128]{2,1,0:T(8,128)(2,1)} %param.18), channel_id=1, source_target_pairs={{0,1},{1,2},{2,3},{3,4},{4,5},{5,6},{6,7},{7,0},{8,9},{9,10},{10,1... | collective-permute-start | bytes 6291464 | tf_op jit(solution)/shard_map/ppermute | solution.py:27
  58.9 99.2 %copy-start.9 = (bf16[4,2048,128]{2,1,0:T(8,128)(2,1)}, bf16[4,2048,128]{2,1,0:T(8,128)(2,1)S(1)}, u32[]{:S(2)}) copy-start(bf16[4,2048,128]{2,1,0:T(8,128)(2,1)S(1)} %collective-permute-done.1) | copy-start | bytes 6291460
  58.9 83.9 %collective-permute-start.2 = (bf16[4,2048,128]{2,1,0:T(8,128)(2,1)S(1)}, bf16[4,2048,128]{2,1,0:T(8,128)(2,1)}, u32[]{:S(2)}, u32[]{:S(2)}) collective-permute-start(bf16[4,2048,128]{2,1,0:T(8,128)(2,1)S(1)} %collective-permute-done.1), channel_id=1, source_target_pairs={{0,1},{1,2},{2,3},{3,4},{4,5},{5,6},{6,7},{7,0},{8,9},{9,10},{10,1... | collective-permute-start | bytes 6291464 | tf_op jit(solution)/shard_map/ppermute | solution.py:27
  60.5 105.5 %collective-permute-start.5 = (bf16[4,2048,128]{2,1,0:T(8,128)(2,1)}, bf16[4,2048,128]{2,1,0:T(8,128)(2,1)}, u32[]{:S(2)}, u32[]{:S(2)}) collective-permute-start(bf16[4,2048,128]{2,1,0:T(8,128)(2,1)} %param.18), channel_id=1, source_target_pairs={{0,7},{1,0},{2,1},{3,2},{4,3},{5,4},{6,5},{7,6},{8,15},{9,8},{10,9... | collective-permute-start | bytes 6291464 | tf_op jit(solution)/shard_map/ppermute | solution.py:28
  142.8 82.7 %collective-permute-start.3 = (bf16[4,2048,128]{2,1,0:T(8,128)(2,1)}, bf16[4,2048,128]{2,1,0:T(8,128)(2,1)}, u32[]{:S(2)}, u32[]{:S(2)}) collective-permute-start(bf16[4,2048,128]{2,1,0:T(8,128)(2,1)} %collective-permute-done.2), channel_id=1, source_target_pairs={{0,1},{1,2},{2,3},{3,4},{4,5},{5,6},{6,7},{7,0},{8,9},{9,10},{10,1... | collective-permute-start | bytes 6291464 | tf_op jit(solution)/shard_map/ppermute | solution.py:27
  158.1 3.9 copy-start.4
  158.1 86.4 %all-to-all-start.1 = ((bf16[16,48,2048]{2,1,0:T(8,128)(2,1)}), bf16[16,48,2048]{2,1,0:T(8,128)(2,1)S(1)}, u32[]{:S(2)}, u32[]{:S(2)}) async-start(bf16[16,48,2048]{2,1,0:T(8,128)(2,1)} %bitcast.7), calls=%async_computation.1 | async-start | bytes 6291456 | tf_op jit(solution)/shard_map/all_to_all | solution.py:112
  161.9 81.4 %copy-start.8 = (f32[128]{0:T(128)S(1)}, f32[128]{0:T(128)}, u32[]{:S(2)}) copy-start(f32[128]{0:T(128)} %param.11) | copy-start | bytes 1540
  161.9 346.4 %all-gather.4.cloned.1.call-start = ((), (), s32[]{:S(2)}) async-start(), calls=%async_computation.3 | async-start | bytes 4718592 | tf_op jit(solution)/shard_map/all_gather | solution.py:98
  162.0 81.1 %collective-permute-start = (bf16[15,128]{1,0:T(8,128)(2,1)S(1)}, bf16[15,128]{1,0:T(8,128)(2,1)S(1)}, u32[]{:S(2)}, u32[]{:S(2)}) collective-permute-start(bf16[15,128]{1,0:T(8,128)(2,1)S(1)} %slice.57), channel_id=1, source_target_pairs={{0,8},{8,16},{16,24},{1,9},{9,17},{17,25},{2,10},{10,18},{18,26},{... | collective-permute-start | bytes 11528 | tf_op jit(solution)/shard_map/ppermute | solution.py:41
  166.0 105.2 %collective-permute-start.6 = (bf16[4,2048,128]{2,1,0:T(8,128)(2,1)}, bf16[4,2048,128]{2,1,0:T(8,128)(2,1)}, u32[]{:S(2)}, u32[]{:S(2)}) collective-permute-start(bf16[4,2048,128]{2,1,0:T(8,128)(2,1)} %collective-permute-done.5), channel_id=1, source_target_pairs={{0,7},{1,0},{2,1},{3,2},{4,3},{5,4},{6,5},{7,6},{8,15},{9,8},{10,9... | collective-permute-start | bytes 6291464 | tf_op jit(solution)/shard_map/ppermute | solution.py:28
  225.5 63.3 %collective-permute-start.4 = (bf16[4,2048,128]{2,1,0:T(8,128)(2,1)}, bf16[4,2048,128]{2,1,0:T(8,128)(2,1)}, u32[]{:S(2)}, u32[]{:S(2)}) collective-permute-start(bf16[4,2048,128]{2,1,0:T(8,128)(2,1)} %collective-permute-done.3), channel_id=1, source_target_pairs={{0,1},{1,2},{2,3},{3,4},{4,5},{5,6},{6,7},{7,0},{8,9},{9,10},{10,1... | collective-permute-start | bytes 6291464 | tf_op jit(solution)/shard_map/ppermute | solution.py:27
  244.5 236.9 %all-to-all-start = ((bf16[8,128,128]{2,1,0:T(8,128)(2,1)}), bf16[8,128,128]{2,1,0:T(8,128)(2,1)S(1)}, u32[]{:S(2)}, u32[]{:S(2)}) async-start(bf16[8,128,128]{2,1,0:T(8,128)(2,1)} %bitcast), calls=%async_computation | async-start | bytes 524288 | tf_op jit(solution)/shard_map/all_to_all | solution.py:95
  271.1 78.0 %copy-start.1 = (bf16[4,4,48,2048]{3,2,0,1:T(8,128)(2,1)}, bf16[4,4,48,2048]{3,2,0,1:T(8,128)(2,1)S(1)}, u32[]{:S(2)}) copy-start(bf16[4,4,48,2048]{3,2,0,1:T(8,128)(2,1)S(1)} %copy.56) | copy-start | bytes 9437188
  271.2 78.0 %collective-permute-start.7 = (bf16[4,2048,128]{2,1,0:T(8,128)(2,1)}, bf16[4,2048,128]{2,1,0:T(8,128)(2,1)S(1)}, u32[]{:S(2)}, u32[]{:S(2)}) collective-permute-start(bf16[4,2048,128]{2,1,0:T(8,128)(2,1)} %collective-permute-done.6), channel_id=1, source_target_pairs={{0,7},{1,0},{2,1},{3,2},{4,3},{5,4},{6,5},{7,6},{8,15},{9,8},{10,9... | collective-permute-start | bytes 6291464 | tf_op jit(solution)/shard_map/ppermute | solution.py:28
  295.5 3.5 copy-start.10
  350.9 106.7 %copy-start.2 = (bf16[4,4,48,2048]{3,2,0,1:T(8,128)(2,1)S(1)}, bf16[4,4,48,2048]{3,2,0,1:T(8,128)(2,1)}, u32[]{:S(2)}) copy-start(bf16[4,4,48,2048]{3,2,0,1:T(8,128)(2,1)} %copy-done.1) | copy-start | bytes 9437188
  481.3 4.4 copy-start.7
  481.3 0.7 copy-start.3
  482.0 40.5 %all-to-all-start.2 = ((bf16[4,192,2048]{2,0,1:T(4,128)(2,1)}), bf16[4,192,2048]{2,0,1:T(4,128)(2,1)S(1)}, u32[]{:S(2)}, u32[]{:S(2)}) async-start(bf16[4,192,2048]{2,0,1:T(4,128)(2,1)} %copy.58), calls=%async_computation.2 | async-start | bytes 6291456 | tf_op jit(solution)/shard_map/all_to_all | solution.py:128
Sparse Core Ops, SparseCore 0:
  9.6 255.6 all-gather.5
  266.9 190.5 all-gather.7
  459.2 49.1 all-gather.3
